TPU v7x, 32 devices: a whole 2x2x4 slice. The times are simulated.
32 devices in a mesh: gr: 2 (over x), sp: 8 (over z, y), tp: 2 (over core).
Axes of the slice: x: 2, y: 2, z: 4, core: 2. Of those that a mesh axis runs over, the one named last changes fastest.
Arguments:
- tokens: bfloat16 [4, 2, 2048, 4096], P('gr', 'tp', 'sp'), may hold values from -6 to 6
- ln_gain: bfloat16 [4096], replicated, may hold values from 0.099609375 to 1.8984375
- w_key: bfloat16 [4096, 256], P('sp'), may hold values from -0.09375 to 0.09375
- w_value: bfloat16 [4096, 256], P('sp'), may hold values from -0.09375 to 0.09375
- queries: bfloat16 [16, 512], P(('gr', 'sp')), may hold values from -6 to 6
- head_shift: float32 [4, 8], replicated
- key_shift: float32 [16, 4096], P(('gr', 'sp'), 'tp')
Outputs:
- kv_cache: bfloat16 [16, 4096, 128], P(('gr', 'sp'), 'tp')
- first_read: float32 [16, 512], P(('gr', 'sp'))
All inputs are finite; a program needn't handle non-finite values.
Results may differ from a plain program's by a relative error of at most 0.0064.
Values may be sent and summed in bfloat16 or wider, within the bound.
A program may use at most 64 MiB of HBM per device.

v0:
```python
import jax
import jax.numpy as jnp
from jax import lax
from jax.sharding import PartitionSpec as P

HD = 64
KVH = 4
GROUP = 8


epsilon = 1e-05


def prefix(shard, axis, combine, identity):
    devices, place = (lax.axis_size(axis), lax.axis_index(axis))
    everything = lax.all_gather(shard, axis)
    start = jnp.broadcast_to(jnp.asarray(identity, shard.dtype), shard.shape)

    def hop(k, before):
        at = devices - 1 - k
        reached = at > place
        new = combine(before, everything[at])
        return jnp.where(reached, new, before)

    return lax.fori_loop(0, devices, hop, start)


def add_columns(normed, segment):
    return jnp.dot(normed, segment, preferred_element_type=jnp.float32)


def by_pair(matrix, seq_count, sub_count):
    shaped = matrix.reshape(seq_count, sub_count, KVH, matrix.shape[1] // KVH)
    return jnp.transpose(shaped, (0, 2, 1, 3)).reshape(
        seq_count * KVH, sub_count, matrix.shape[1] // KVH
    )


def combine_sums(earlier, later):
    return earlier + later


def local(tokens, ln_gain, w_key, w_value, queries, head_shift, key_shift):
    seq_count = tokens.shape[0]
    sub_count = tokens.shape[2]
    width = tokens.shape[3]
    flat_rows = tokens.reshape(seq_count * sub_count, width).astype(jnp.float32)
    row_mean = jnp.mean(flat_rows, axis=1, keepdims=True)
    centred = flat_rows - row_mean
    row_var = jnp.mean(centred * centred, axis=1, keepdims=True)
    normed = (centred * lax.rsqrt(row_var + epsilon) * ln_gain.astype(jnp.float32)).astype(
        jnp.bfloat16
    )

    def add_one(segment):
        return add_columns(normed, segment)

    keys = add_one(lax.all_gather(w_key, "sp", axis=0, tiled=True)).astype(jnp.bfloat16)
    key_part = lax.all_to_all(
        by_pair(keys, seq_count, sub_count), "sp", split_axis=0, concat_axis=1, tiled=True
    )
    values = add_one(lax.all_gather(w_value, "sp", axis=0, tiled=True)).astype(jnp.bfloat16)
    value_part = lax.all_to_all(
        by_pair(values, seq_count, sub_count), "sp", split_axis=0, concat_axis=1, tiled=True
    )
    cache_here = jnp.concatenate([key_part, value_part], axis=2)
    own_keys = cache_here[0, :, :HD]
    own_values = cache_here[0, :, HD:]
    kv_head = lax.axis_index("sp") % KVH
    picker = (jnp.arange(KVH) == kv_head).astype(jnp.float32)
    head_row = jnp.sum(picker[:, None] * head_shift, axis=0)
    query = queries.reshape(GROUP, HD)
    logits = jnp.einsum("gd,jd->gj", query, own_keys, preferred_element_type=jnp.float32) * HD ** (
        -0.5
    )
    logits = logits + head_row[:, None] + key_shift[0][None, :]
    log_beta = jax.nn.log_sigmoid(logits)
    log_keep = log_beta - logits
    within = lax.cumsum(log_keep, axis=1, reverse=True) - log_keep
    local_weight = jnp.exp(log_beta + within).astype(jnp.bfloat16)
    section_part = jnp.dot(local_weight, own_values, preferred_element_type=jnp.float32)
    section_total = jnp.sum(log_keep, axis=1)
    carry = prefix(section_total, "tp", combine_sums, jnp.zeros_like(section_total))
    first_read = lax.psum(jnp.exp(carry)[:, None] * section_part, "tp")
    return (cache_here, first_read.reshape(1, GROUP * HD))


def solution(mesh):
    in_specs = (
        P("gr", "tp", "sp", None),
        P(),
        P("sp", None),
        P("sp", None),
        P(("gr", "sp"), None),
        P(),
        P(("gr", "sp"), "tp"),
    )
    out_specs = (P(("gr", "sp"), "tp", None), P(("gr", "sp"), None))
    return jax.shard_map(local, mesh=mesh, in_specs=in_specs, out_specs=out_specs, check_vma=False)
```

profile of v0, /device:TPU:0, one launch (start us, length us, event | category | flops | bytes accessed | tf_op | source)
XLA Modules:
  0.0 148.5 jit_solution(7255145093964798243)
XLA Ops:
  7.2 0.7 all-gather.4.cloned.1.call-update
  7.9 0.7 all-gather.6.cloned.1.call-update
  8.7 3.0 %convert_reduce_fusion = f32[2,256]{1,0:T(2,128)S(1)} fusion(bf16[2,1,256,4096]{3,2,1,0:T(8,128)(2,1)} %param.9), kind=kLoop, calls=%fused_computation.7 | loop fusion | flops 4193792 | bytes 4196352 | tf_op jit(solution)/shard_map/reduce_sum | solution.py:48
  11.7 0.4 copy-done
  12.1 1.2 multiply_reduce_fusion
  13.5 0.6 dynamic-slice
  14.9 6.4 %fusion.2 = bf16[512,4096]{1,0:T(8,128)(2,1)} fusion(bf16[2,1,256,4096]{3,2,1,0:T(8,128)(2,1)} %param.9, f32[4096]{0:T(1024)S(1)} %convert_element_type.35, f32[512]{0:T(512)S(1)} %bitcast.65, f32[512]{0:T(512)S(1)} %bitcast.66), kind=kLoop, calls=%fused_computation.5 | loop fusion | flops 10485760 | bytes 8409088 | tf_op jit(solution)/shard_map/convert_element_type | solution.py:51
  21.3 40.7 %all-gather.4.cloned.1.call-done = bf16[4096,256]{1,0:T(8,128)(2,1)} async-done(((bf16[512,256]{1,0:T(8,128)(2,1)}), bf16[4096,256]{1,0:T(8,128)(2,1)}) %all-gather.4.cloned.1.call-update) | async-done | bytes 2097168 | tf_op jit(solution)/shard_map/all_gather | solution.py:58
  61.9 4.1 %convolution_convert_fusion.1 = bf16[512,256]{1,0:T(8,128)(2,1)S(1)} fusion(bf16[512,4096]{1,0:T(8,128)(2,1)} %fusion.2, bf16[4096,256]{1,0:T(8,128)(2,1)} %all-gather.4.cloned.1.call-done), kind=kOutput, calls=%fused_computation.13 | convolution fusion | flops 1073872896 | bytes 6553600 | tf_op jit(solution)/shard_map/dot_general | solution.py:29
  66.3 0.7 copy.16
  67.0 3.4 %all-to-all-start = ((bf16[8,256,64]{1,2,0:T(8,128)(2,1)}), bf16[8,256,64]{1,2,0:T(8,128)(2,1)S(1)}, u32[]{:S(2)}, u32[]{:S(2)}) async-start(bf16[8,256,64]{1,2,0:T(8,128)(2,1)} %bitcast.2), calls=%async_computation | async-start | bytes 524288 | tf_op jit(solution)/shard_map/all_to_all | solution.py:59
  70.4 44.2 %all-gather.6.cloned.1.call-done = bf16[4096,256]{1,0:T(8,128)(2,1)} async-done(((bf16[512,256]{1,0:T(8,128)(2,1)}), bf16[4096,256]{1,0:T(8,128)(2,1)}) %all-gather.6.cloned.1.call-update) | async-done | bytes 2097168 | tf_op jit(solution)/shard_map/all_gather | solution.py:62
  114.7 4.1 %convolution_convert_fusion = bf16[512,256]{1,0:T(8,128)(2,1)S(1)} fusion(bf16[512,4096]{1,0:T(8,128)(2,1)} %fusion.2, bf16[4096,256]{1,0:T(8,128)(2,1)} %all-gather.6.cloned.1.call-done), kind=kOutput, calls=%fused_computation.12 | convolution fusion | flops 1073872896 | bytes 6553600 | tf_op jit(solution)/shard_map/dot_general | solution.py:29
  119.0 0.7 copy.19
  119.7 3.4 %all-to-all-start.1 = ((bf16[8,256,64]{1,2,0:T(8,128)(2,1)}), bf16[8,256,64]{1,2,0:T(8,128)(2,1)S(1)}, u32[]{:S(2)}, u32[]{:S(2)}) async-start(bf16[8,256,64]{1,2,0:T(8,128)(2,1)} %bitcast.4), calls=%async_computation.1 | async-start | bytes 524288 | tf_op jit(solution)/shard_map/all_to_all | solution.py:63
  123.4 0.2 fusion.15
  123.5 9.9 %reduce-window.6 = f32[8,16,128]{2,1,0:T(8,128)S(1)} reduce-window(f32[8,16,128]{2,1,0:T(8,128)S(1)} %copy.22, f32[]{:T(128)} %constant.62.clone.1), window={size=1x1x128 pad=0_0x0_0x0_127}, to_apply=%region_6.7 | reduce-window | flops 2080768 | bytes 131076 | tf_op jit(solution)/shard_map/reduce-window
  133.6 0.2 reduce-window.9
  133.8 0.2 dynamic-update-slice
  134.0 2.4 %all-reduce = f32[16]{0:T(128)S(1)} all-reduce(f32[16]{0:T(128)S(1)} %dynamic-update-slice), channel_id=2, replica_groups=mesh['gr'=2,'sp'=8,'tp'=2] {'tp'}, use_global_device_ids=true, to_apply=%add | all-reduce | flops 16 | bytes 128
  136.7 0.2 convolution_multiply_fusion.1
  137.0 3.0 %psum.7 = f32[1,512]{1,0:T(1,128)} all-reduce(f32[1,512]{1,0:T(1,128)S(1)} %reshape.96), channel_id=1, replica_groups=mesh['gr'=2,'sp'=8,'tp'=2] {'tp'}, use_global_device_ids=true, to_apply=%region_8.9 | all-reduce | flops 512 | bytes 4096 | tf_op jit(solution)/shard_map/psum | solution.py:84
  140.3 0.2 copy.17
  140.7 1.0 copy.24
  (47 shorter events, 1.9 us)
Async XLA Ops:
  7.2 54.8 %all-gather.4.cloned.1.call-start = ((), (), s32[]{:S(2)}) async-start(), calls=%async_computation.2 | async-start | bytes 2359296 | tf_op jit(solution)/shard_map/all_gather | solution.py:58
  7.9 106.8 %all-gather.6.cloned.1.call-start = ((), (), s32[]{:S(2)}) async-start(), calls=%async_computation.3 | async-start | bytes 2359296 | tf_op jit(solution)/shard_map/all_gather | solution.py:62
  8.7 3.5 %copy-start = (bf16[2,1,256,4096]{3,2,1,0:T(8,128)(2,1)S(1)}, bf16[2,1,256,4096]{3,2,1,0:T(8,128)(2,1)}, u32[]{:S(2)}) copy-start(bf16[2,1,256,4096]{3,2,1,0:T(8,128)(2,1)} %param.9) | copy-start | bytes 12582916
  8.7 4.7 %copy-start.1 = (bf16[4096]{0:T(1024)(128)(2,1)S(1)}, bf16[4096]{0:T(1024)(128)(2,1)}, u32[]{:S(2)}) copy-start(bf16[4096]{0:T(1024)(128)(2,1)} %param.10) | copy-start | bytes 24580
  8.7 4.7 %copy-start.3 = (bf16[1,512]{1,0:T(2,128)(2,1)S(1)}, bf16[1,512]{1,0:T(2,128)(2,1)}, u32[]{:S(2)}) copy-start(bf16[1,512]{1,0:T(2,128)(2,1)} %param.13) | copy-start | bytes 3076
  8.7 4.8 %copy-start.5 = (u32[32]{0:T(128)S(1)}, u32[32]{0:T(128)}, u32[]{:S(2)}) copy-start(u32[32]{0:T(128)} %constant.76) | copy-start | bytes 388
  8.7 6.1 %copy-start.4 = (f32[4,8]{1,0:T(4,128)S(1)}, f32[4,8]{1,0:T(4,128)}, u32[]{:S(2)}) copy-start(f32[4,8]{1,0:T(4,128)} %param.14) | copy-start | bytes 388
  67.0 52.7 %all-to-all-start = ((bf16[8,256,64]{1,2,0:T(8,128)(2,1)}), bf16[8,256,64]{1,2,0:T(8,128)(2,1)S(1)}, u32[]{:S(2)}, u32[]{:S(2)}) async-start(bf16[8,256,64]{1,2,0:T(8,128)(2,1)} %bitcast.2), calls=%async_computation | async-start | bytes 524288 | tf_op jit(solution)/shard_map/all_to_all | solution.py:59
  70.4 52.8 %copy-start.2 = (f32[1,2048]{1,0:T(1,128)S(1)}, f32[1,2048]{1,0:T(1,128)}, u32[]{:S(2)}) copy-start(f32[1,2048]{1,0:T(1,128)} %param.15) | copy-start | bytes 24580
  119.7 17.0 %all-to-all-start.1 = ((bf16[8,256,64]{1,2,0:T(8,128)(2,1)}), bf16[8,256,64]{1,2,0:T(8,128)(2,1)S(1)}, u32[]{:S(2)}, u32[]{:S(2)}) async-start(bf16[8,256,64]{1,2,0:T(8,128)(2,1)} %bitcast.4), calls=%async_computation.1 | async-start | bytes 524288 | tf_op jit(solution)/shard_map/all_to_all | solution.py:63
Sparse Core Ops, SparseCore 0:
  10.1 51.7 all-gather.3
  64.1 50.5 all-gather.5
where the time goes:
time: 149 us
  waiting for transfers between devices  86.3 us (58%)
  other arithmetic  21.1 us (14%)
  between operations  15 us (10%)
  matrix products  8.56 us (6%)
  starting transfers between devices  6.9 us (5%)
  blocking collectives  5.49 us (4%)
  local copies, waits for them, and re-layouts  5.14 us (3%)
    all_gather x1, waiting for transfers between devices, local(): lax.all_gather(w_value, 'sp', axis=0, tiled=True)  44.2 us
    all_gather x1, waiting for transfers between devices, local(): lax.all_gather(w_key, 'sp', axis=0, tiled=True)  40.7 us
    another operation x2, other arithmetic  10.1 us
    dot_general x2, matrix products, add_columns(): return jnp.dot(normed, segment, preferred_element_type=jnp.float32)  8.23 us
    convert_element_type x1, other arithmetic, local(): (centred * lax.rsqrt(row_var + epsilon) * ln_gain.astype(jnp.float32)).as...  6.39 us
    all_to_all x1, starting transfers between devices, local(): lax.all_to_all(by_pair(values, seq_count, sub_count), 'sp', split_axis=0,...  3.41 us
    all_to_all x1, starting transfers between devices, local(): lax.all_to_all(by_pair(keys, seq_count, sub_count), 'sp', split_axis=0, c...  3.41 us
    psum x1, blocking collectives, local(): first_read = lax.psum(jnp.exp(carry)[:, None] * section_part, 'tp')  3.04 us
  transfers between devices with their start and end apart: 4, of which 2 were waited for; matrix products, arithmetic and copies ran while one was open for 22% of the time, Pallas kernels for 0%

commit v1 on v0

v1 whole, which is shorter than its diff:
```python
import functools

import jax
import jax.numpy as jnp
from jax import lax
from jax.experimental import pallas as pl
from jax.experimental.pallas import tpu as pltpu
from jax.sharding import PartitionSpec as P

epsilon = 1e-05
STAGES = 4
MESH = pl.DeviceIdType.MESH


def layout(mesh):
    sp, gr, tp = mesh.shape["sp"], mesh.shape["gr"], mesh.shape["tp"]
    inner = 1
    while inner * inner * 4 <= sp and sp % (inner * 2) == 0:
        inner *= 2
    return sp // inner, inner, gr, tp


def body(
    grid, head_size,
    tokens, gain, w_key, w_value, queries, head_shift, key_shift,
    cache, read,
    raw, normed, weights, acc, outgoing, incoming, totals, parts,
    send_sem, recv_sem, load_sem,
):
    depth, inner, groups, sections = grid
    seats = depth * inner
    seat, group, section = lax.axis_index("sp"), lax.axis_index("gr"), lax.axis_index("tp")
    lane, place = seat // inner, seat % inner
    rows, width = raw.shape
    shard, columns = w_key.shape
    piece = shard // (groups * sections)
    kv_heads, heads = head_shift.shape
    seqs = seats // kv_heads
    sub = rows // seqs
    half = sub // 2
    stage_rows = rows // STAGES

    sent = []

    def push(source, target, **where):
        at = len(sent)
        copy = pltpu.make_async_remote_copy(
            src_ref=source, dst_ref=target, send_sem=send_sem.at[at], recv_sem=recv_sem.at[at],
            device_id=where, device_id_type=MESH,
        )
        copy.start()
        sent.append(copy)
        return copy

    own = pl.ds(pl.multiple_of(seat * shard, shard), shard)
    loads = []
    for at, source in enumerate((w_key, w_value)):
        loads.append(pltpu.make_async_copy(source, weights.at[at, own], load_sem.at[at]))
        loads[-1].start()
    fills = []
    for at in range(STAGES):
        block = pl.ds(at * stage_rows, stage_rows)
        fills.append(pltpu.make_async_copy(tokens.at[block], raw.at[block], load_sem.at[2 + at]))
        fills[-1].start()

    def seat_at(k, j):
        return lax.rem(lane + depth - k, depth) * inner + lax.rem(place + inner - j, inner)

    barrier = pltpu.get_barrier_semaphore()
    for i in range(1, seats):
        pl.semaphore_signal(barrier, 1, device_id={"sp": lax.rem(seat + i, seats)}, device_id_type=MESH)
    for i in range(1, groups):
        pl.semaphore_signal(barrier, 1, device_id={"gr": lax.rem(group + i, groups)}, device_id_type=MESH)
    for i in range(1, sections):
        pl.semaphore_signal(barrier, 1, device_id={"tp": lax.rem(section + i, sections)}, device_id_type=MESH)
    pl.semaphore_wait(barrier, seats + groups + sections - 3)

    def block_of(m, k, j, g):
        share = lax.rem(group + groups - g, groups) * sections + section
        start = seat_at(k, j) * shard + share * piece
        return weights.at[m, pl.ds(pl.multiple_of(start, piece), piece)]

    got = {}
    crossed = {}

    def along_lane(m):
        for k in range(1, depth):
            to = lax.rem(lane + k, depth) * inner + place
            block = block_of(m, 0, 0, 0)
            got[m, k, 0, 0] = push(block, block, sp=to)

    def along_place(m, k, g):
        for j in range(1, inner):
            to = lane * inner + lax.rem(place + j, inner)
            block = block_of(m, k, 0, g)
            got[m, k, j, g] = push(block, block, sp=to)

    def along_group(m, k, j):
        if k == 0 and j == 0:
            return
        for g in range(1, groups):
            block = block_of(m, k, j, 0)
            got[m, k, j, g] = push(block, block, gr=lax.rem(group + g, groups))

    def along_section(m, k, j, g):
        if k == 0 and j == 0:
            return
        block = block_of(m, k, j, g)
        for t in range(1, sections):
            copy = push(block, block, tp=lax.rem(section + t, sections))
            crossed.setdefault((m, k), []).append(copy)

    def normalise(at):
        fills[at].wait()
        step = 32

        @pl.loop(0, stage_rows // step)
        def _(i):
            here = pl.ds(pl.multiple_of(at * stage_rows + i * step, step), step)
            x = raw[here, :].astype(jnp.float32)
            mean = jnp.mean(x, axis=1, keepdims=True)
            centred = x - mean
            var = jnp.mean(centred * centred, axis=1, keepdims=True)
            scale = gain[...].astype(jnp.float32)
            normed[here, :] = (centred * lax.rsqrt(var + epsilon) * scale).astype(jnp.bfloat16)

    def multiply(m, k):
        for copy in crossed.get((m, k), ()):
            copy.wait_recv()
        span = inner * shard
        start = pl.multiple_of(lax.rem(lane + depth - k, depth) * span, span)
        out = jnp.dot(normed[:, pl.ds(start, span)], weights[m, pl.ds(start, span), :], preferred_element_type=jnp.float32)
        if k == 0:
            acc[...] = out
        else:
            acc[...] += out

    swapped = {}

    def exchange(m):
        for pair in range(seats):
            seq, head = pair // kv_heads, pair % kv_heads
            cut = slice(head * head_size, (head + 1) * head_size)
            first = acc[seq * sub:seq * sub + half, cut]
            second = acc[seq * sub + half:(seq + 1) * sub, cut]
            outgoing[m, pair] = jnp.concatenate([first, second], axis=1).astype(jnp.bfloat16)
        for i in range(1, seats):
            to = lax.rem(seat + i, seats)
            swapped[m, i] = push(outgoing.at[m, to], incoming.at[m, seat], sp=to)
        incoming[m, pl.ds(seat, 1)] = outgoing[m, pl.ds(seat, 1)]

    loads[0].wait()
    along_place(0, 0, 0)
    along_lane(0)
    loads[1].wait()
    along_lane(1)
    for g in range(groups):
        along_place(1, 0, g)
    normalise(0)
    for j in range(1, inner):
        got[0, 0, j, 0].wait_recv()
        along_group(0, 0, j)
        along_section(0, 0, j, 0)
    normalise(1)
    for k in range(1, depth):
        got[0, k, 0, 0].wait_recv()
        along_place(0, k, 0)
        along_group(0, k, 0)
        along_section(0, k, 0, 0)
        got[1, k, 0, 0].wait_recv()
        along_group(1, k, 0)
        along_place(1, k, 0)
        along_section(1, k, 0, 0)
        if k == 1:
            normalise(2)
    for k in range(1, depth):
        for j in range(1, inner):
            got[0, k, j, 0].wait_recv()
            along_group(0, k, j)
            along_section(0, k, j, 0)
        for g in range(1, groups):
            got[1, k, 0, g].wait_recv()
            along_place(1, k, g)
            along_section(1, k, 0, g)
    for at in range(3, STAGES):
        normalise(at)
    for m in range(2):
        for k in range(depth):
            for j in range(inner):
                for g in range(groups):
                    last = g > 0 if m == 0 else j > 0
                    if last and not (k == 0 and j == 0):
                        got[m, k, j, g].wait_recv()
                        along_section(m, k, j, g)
            if k > 0:
                multiply(m, k - 1)
        multiply(m, depth - 1)
        exchange(m)

    query = queries[...].astype(jnp.float32)
    query = jnp.concatenate([query[:, g * head_size:(g + 1) * head_size] for g in range(heads)], axis=0)
    blank = jnp.zeros_like(query)
    query = jnp.concatenate(
        [jnp.concatenate([query, blank], axis=1), jnp.concatenate([blank, query], axis=1)], axis=0
    ).astype(jnp.bfloat16)
    mine = lax.broadcasted_iota(jnp.int32, (kv_heads, heads), 0) == lax.rem(seat, kv_heads)
    shift = jnp.sum(jnp.where(mine, head_shift[...], 0.0), axis=0, keepdims=True)
    eye = lax.broadcasted_iota(jnp.int32, (heads, heads), 0) == lax.broadcasted_iota(jnp.int32, (heads, heads), 1)
    shift = jnp.sum(jnp.where(eye, jnp.broadcast_to(shift, (heads, heads)), 0.0), axis=1, keepdims=True)
    later = (
        lax.broadcasted_iota(jnp.int32, (half, half), 0) > lax.broadcasted_iota(jnp.int32, (half, half), 1)
    ).astype(jnp.float32)

    for i in range(1, seats):
        swapped[0, i].wait_recv()
    keys = incoming[0].reshape(seats * half, 2 * head_size)
    logits = lax.dot_general(query, keys, (((1,), (1,)), ((), ())), preferred_element_type=jnp.float32)
    logits = logits * head_size ** (-0.5)
    betas, keeps = [], []
    for at in range(2 * seats):
        q, h = at // 2, at % 2
        z = logits[h * heads:(h + 1) * heads, q * half:(q + 1) * half]
        z = z + shift + key_shift[:, at * half:(at + 1) * half]
        tail = jnp.log1p(jnp.exp(-jnp.abs(z)))
        betas.append(jnp.minimum(z, 0.0) - tail)
        keeps.append(jnp.minimum(-z, 0.0) - tail)
    within = jnp.dot(
        jnp.concatenate(keeps, axis=0), later, preferred_element_type=jnp.float32, precision=lax.Precision.HIGHEST
    )
    running = jnp.zeros((heads, 1), jnp.float32)
    local = [None] * (2 * seats)
    for at in reversed(range(2 * seats)):
        local[at] = jnp.exp(betas[at] + within[at * heads:(at + 1) * heads] + running)
        running = running + jnp.sum(keeps[at], axis=1, keepdims=True)
    local = jnp.concatenate(
        [jnp.concatenate(local[0::2], axis=1), jnp.concatenate(local[1::2], axis=1)], axis=0
    ).astype(jnp.bfloat16)
    totals[section] = jnp.broadcast_to(running, totals.shape[1:])
    arrivals = [
        push(totals.at[section], totals.at[section], tp=lax.rem(section + t, sections)) for t in range(1, sections)
    ]
    for copy in arrivals:
        copy.wait_recv()
    carry = jnp.zeros((heads, head_size), jnp.float32)
    for t in reversed(range(sections)):
        carry = carry + jnp.where(section < t, totals[t][:, :head_size], 0.0)
    carry = jnp.exp(carry)

    for i in range(1, seats):
        swapped[1, i].wait_recv()
    values = incoming[1].reshape(seats * half, 2 * head_size)
    part = jnp.dot(local, values, preferred_element_type=jnp.float32)
    part = carry * (part[:heads, :head_size] + part[heads:, head_size:])
    parts[section] = jnp.concatenate([part, part], axis=1)
    arrivals = [
        push(parts.at[section], parts.at[section], tp=lax.rem(section + t, sections)) for t in range(1, sections)
    ]
    for q in range(seats):
        for h in range(2):
            cut = slice(h * head_size, (h + 1) * head_size)
            start = (2 * q + h) * half
            cache[0, start:start + half, :] = jnp.concatenate([incoming[0, q][:, cut], incoming[1, q][:, cut]], axis=1)
    for copy in arrivals:
        copy.wait_recv()
    total = parts[0]
    for t in range(1, sections):
        total = total + parts[t]
    for g in range(heads):
        read[:, g * head_size:(g + 1) * head_size] = total[g:g + 1, :head_size]
    for copy in sent:
        copy.wait_send()


def copies(grid):
    depth, inner, groups, sections = grid
    pieces = depth * inner * groups
    gather = pieces + (pieces - groups) * (sections - 1)
    return 2 * gather + 2 * (depth * inner - 1) + 2 * (sections - 1)


def local(grid, tokens, ln_gain, w_key, w_value, queries, head_shift, key_shift):
    depth, inner, groups, sections = grid
    seats = depth * inner
    seqs, _, sub, width = tokens.shape
    rows = seqs * sub
    columns = w_key.shape[1]
    kv_heads, heads = head_shift.shape
    head_size = columns // kv_heads
    vmem = pl.BlockSpec(memory_space=pltpu.VMEM)
    hbm = pl.BlockSpec(memory_space=pl.ANY)
    count = copies(grid)
    cache, read = pl.pallas_call(
        functools.partial(body, grid, head_size),
        out_shape=(
            jax.ShapeDtypeStruct((1, seats * sub, 2 * head_size), jnp.bfloat16),
            jax.ShapeDtypeStruct((1, heads * head_size), jnp.float32),
        ),
        in_specs=[hbm, vmem, hbm, hbm, vmem, vmem, vmem],
        out_specs=(vmem, vmem),
        scratch_shapes=[
            pltpu.VMEM((rows, width), jnp.bfloat16),
            pltpu.VMEM((rows, width), jnp.bfloat16),
            pltpu.VMEM((2, width, columns), jnp.bfloat16),
            pltpu.VMEM((rows, columns), jnp.float32),
            pltpu.VMEM((2, seats, sub // 2, 2 * head_size), jnp.bfloat16),
            pltpu.VMEM((2, seats, sub // 2, 2 * head_size), jnp.bfloat16),
            pltpu.VMEM((sections, heads, 2 * head_size), jnp.float32),
            pltpu.VMEM((sections, heads, 2 * head_size), jnp.float32),
            pltpu.SemaphoreType.DMA((count,)),
            pltpu.SemaphoreType.DMA((count,)),
            pltpu.SemaphoreType.DMA((2 + STAGES,)),
        ],
        compiler_params=pltpu.CompilerParams(
            collective_id=0, has_side_effects=True, vmem_limit_bytes=60 * 1024 * 1024
        ),
    )(tokens.reshape(rows, width), ln_gain.reshape(1, width), w_key, w_value, queries, head_shift, key_shift)
    return cache, read


def solution(mesh):
    in_specs = (
        P("gr", "tp", "sp", None),
        P(),
        P("sp", None),
        P("sp", None),
        P(("gr", "sp"), None),
        P(),
        P(("gr", "sp"), "tp"),
    )
    out_specs = (P(("gr", "sp"), "tp", None), P(("gr", "sp"), None))
    return jax.shard_map(
        functools.partial(local, layout(mesh)), mesh=mesh, in_specs=in_specs, out_specs=out_specs, check_vma=False
    )
```

time: 149 us -> 52.1 us (0.35)
  waiting for transfers between devices: 86.3 us -> 0 us
  Pallas kernels: 0 us -> 46.7 us
  other arithmetic: 21.1 us -> 0 us
  between operations: 15 us -> 0.64 us
  matrix products: 8.56 us -> 0 us
  starting transfers between devices: 6.9 us -> 0 us
  blocking collectives: 5.49 us -> 0 us
    all_gather x2 -> x0, waiting for transfers between devices: 84.9 us -> none  [the longest x1 44.2 us: local(): lax.all_gather(w_value, 'sp', axis=0, tiled=True)]
    pallas_call x0 -> x1, Pallas kernels: none -> 46.7 us  [local(): pl.pallas_call(functools.partial(body, grid, head_size), out_shape=(jax.S...]
    another operation x2 -> x0, other arithmetic: 10.1 us -> none
    dot_general x4 -> x0, matrix products: 8.56 us -> none  [the longest x2 8.23 us: add_columns(): return jnp.dot(normed, segment, preferred_element_type=jnp.float32)]
    all_to_all x2 -> x0, starting transfers between devices: 6.83 us -> none  [the longest x1 3.41 us: local(): lax.all_to_all(by_pair(values, seq_count, sub_count), 'sp', split_axis=0,...]
    convert_element_type x3 -> x0, other arithmetic: 6.4 us -> none  [the longest x1 6.39 us: local(): (centred * lax.rsqrt(row_var + epsilon) * ln_gain.astype(jnp.float32)).as...]
    reduce_sum x4 -> x0, other arithmetic: 4.45 us -> none  [the longest x1 2.96 us: local(): row_mean = jnp.mean(flat_rows, axis=1, keepdims=True)]
    psum x1 -> x0, blocking collectives: 3.04 us -> none  [local(): first_read = lax.psum(jnp.exp(carry)[:, None] * section_part, 'tp')]
  transfers between devices with their start and end apart: 4 -> 0, of which waited for: 2 -> 0; matrix products, arithmetic and copies ran while one was open for 22% -> 0% of each run, Pallas kernels for 0% -> 0%
where the time goes in v1:
time: 52.1 us; the launch traced here: 51.7 us
  Pallas kernels  46.7 us (90%)
  local copies, waits for them, and re-layouts  4.43 us (9%)
  between operations  0.64 us (1%)
    pallas_call x1, Pallas kernels, local(): pl.pallas_call(functools.partial(body, grid, head_size), out_shape=(jax.S...  46.7 us
    unnamed x2, local copies, waits for them, and re-layouts  3.12 us
    reshape x1, local copies, waits for them, and re-layouts, local(): ln_gain.reshape(1, width)  1.31 us

profile of v1, /device:TPU:0, one launch (start us, length us, event | category | flops | bytes accessed | tf_op | source)
XLA Modules:
  0.0 51.7 jit_solution(9641908226597882483)
XLA Ops:
  0.6 1.3 %reshape.11.gain = bf16[1,4096]{1,0:T(2,128)(2,1)} reshape(bf16[4096]{0:T(1024)(128)(2,1)} %param.8) | data formatting | bytes 16384 | tf_op jit(solution)/shard_map/reshape | solution.py:316
  1.9 46.7 %shard_map.86 = (bf16[1,2048,128]{2,1,0:T(8,128)(2,1)}, f32[1,512]{1,0:T(1,128)}) custom-call(bf16[512,4096]{1,0:T(8,128)(2,1)} %bitcast.1, bf16[1,4096]{1,0:T(2,128)(2,1)} %reshape.11.gain, bf16[512,256]{1,0:T(8,128)(2,1)} %w_key.1, bf16[512,256]{1,0:T(8,128)(2,1)} %w_value.1, bf16[1,512]{1,0:T(2,128)(2,1)} %queries.1, f32[4,8]{1,0:T(4,128)} %head_shift.1, ...), custom_call_target="tpu_custom_call" | custom-call | tf_op jit(solution)/shard_map/pallas_call | solution.py:292
  48.6 1.9 %copy.11 = bf16[1,2048,128]{2,1,0:T(8,128)(2,1)} copy(bf16[1,2048,128]{2,1,0:T(8,128)(2,1)} %get-tuple-element.4) | data formatting | bytes 1048576
  50.5 1.3 %copy.12 = f32[1,512]{1,0:T(1,128)} copy(f32[1,512]{1,0:T(1,128)} %get-tuple-element.5) | data formatting | bytes 4096

commit v2 on v1

--- a/solution.py
+++ b/solution.py
@@ -9,6 +9,9 @@
 
 epsilon = 1e-05
 STAGES = 4
+NORM_AT = (0.5, 2.6, 3.1, 5.1)
+LAG, LANE, HOP, CROSS = 3.0, 1.0, 2.5, 1.0
+ORDERS = ((0, 0, 0, 0), (1, 1, 1, 1))
 MESH = pl.DeviceIdType.MESH
 
 
@@ -110,6 +113,41 @@
             copy = push(block, block, tp=lax.rem(section + t, sections))
             crossed.setdefault((m, k), []).append(copy)
 
+    def first(m, k):
+        if k > 0:
+            got[m, k, 0, 0].wait_recv()
+        if ORDERS[m][k % len(ORDERS[m])]:
+            along_group(m, k, 0)
+            along_place(m, k, 0)
+        else:
+            along_place(m, k, 0)
+            along_group(m, k, 0)
+        along_section(m, k, 0, 0)
+        if ORDERS[m][k % len(ORDERS[m])] and k == 0:
+            second(m, k)
+
+    def second(m, k):
+        if ORDERS[m][k % len(ORDERS[m])]:
+            for g in range(1, groups):
+                if k > 0:
+                    got[m, k, 0, g].wait_recv()
+                along_place(m, k, g)
+                along_section(m, k, 0, g)
+        else:
+            for j in range(1, inner):
+                got[m, k, j, 0].wait_recv()
+                along_group(m, k, j)
+                along_section(m, k, j, 0)
+
+    def third(m, k):
+        if ORDERS[m][k % len(ORDERS[m])]:
+            lasts = [(j, g) for j in range(1, inner) for g in range(groups)]
+        else:
+            lasts = [(j, g) for j in range(inner) for g in range(1, groups) if k > 0 or j > 0]
+        for j, g in lasts:
+            got[m, k, j, g].wait_recv()
+            along_section(m, k, j, g)
+
     def normalise(at):
         fills[at].wait()
         step = 32
@@ -121,7 +159,7 @@
             mean = jnp.mean(x, axis=1, keepdims=True)
             centred = x - mean
             var = jnp.mean(centred * centred, axis=1, keepdims=True)
-            scale = gain[...].astype(jnp.float32)
+            scale = gain[...].astype(jnp.float32).reshape(1, width)
             normed[here, :] = (centred * lax.rsqrt(var + epsilon) * scale).astype(jnp.bfloat16)
 
     def multiply(m, k):
@@ -131,9 +169,9 @@
         start = pl.multiple_of(lax.rem(lane + depth - k, depth) * span, span)
         out = jnp.dot(normed[:, pl.ds(start, span)], weights[m, pl.ds(start, span), :], preferred_element_type=jnp.float32)
         if k == 0:
-            acc[...] = out
+            acc[m] = out
         else:
-            acc[...] += out
+            acc[m] += out
 
     swapped = {}
 
@@ -141,8 +179,8 @@
         for pair in range(seats):
             seq, head = pair // kv_heads, pair % kv_heads
             cut = slice(head * head_size, (head + 1) * head_size)
-            first = acc[seq * sub:seq * sub + half, cut]
-            second = acc[seq * sub + half:(seq + 1) * sub, cut]
+            first = acc[m, seq * sub:seq * sub + half, cut]
+            second = acc[m, seq * sub + half:(seq + 1) * sub, cut]
             outgoing[m, pair] = jnp.concatenate([first, second], axis=1).astype(jnp.bfloat16)
         for i in range(1, seats):
             to = lax.rem(seat + i, seats)
@@ -150,52 +188,26 @@
         incoming[m, pl.ds(seat, 1)] = outgoing[m, pl.ds(seat, 1)]
 
     loads[0].wait()
-    along_place(0, 0, 0)
+    first(0, 0)
     along_lane(0)
     loads[1].wait()
     along_lane(1)
-    for g in range(groups):
-        along_place(1, 0, g)
-    normalise(0)
-    for j in range(1, inner):
-        got[0, 0, j, 0].wait_recv()
-        along_group(0, 0, j)
-        along_section(0, 0, j, 0)
-    normalise(1)
-    for k in range(1, depth):
-        got[0, k, 0, 0].wait_recv()
-        along_place(0, k, 0)
-        along_group(0, k, 0)
-        along_section(0, k, 0, 0)
-        got[1, k, 0, 0].wait_recv()
-        along_group(1, k, 0)
-        along_place(1, k, 0)
-        along_section(1, k, 0, 0)
-        if k == 1:
-            normalise(2)
-    for k in range(1, depth):
-        for j in range(1, inner):
-            got[0, k, j, 0].wait_recv()
-            along_group(0, k, j)
-            along_section(0, k, j, 0)
-        for g in range(1, groups):
-            got[1, k, 0, g].wait_recv()
-            along_place(1, k, g)
-            along_section(1, k, 0, g)
-    for at in range(3, STAGES):
-        normalise(at)
+    first(1, 0)
+    steps = [(NORM_AT[at], "norm", normalise, (at,)) for at in range(STAGES)]
     for m in range(2):
+        end = 0.0
         for k in range(depth):
-            for j in range(inner):
-                for g in range(groups):
-                    last = g > 0 if m == 0 else j > 0
-                    if last and not (k == 0 and j == 0):
-                        got[m, k, j, g].wait_recv()
-                        along_section(m, k, j, g)
+            base = m * LAG + k * LANE
             if k > 0:
-                multiply(m, k - 1)
-        multiply(m, depth - 1)
-        exchange(m)
+                steps.append((base, "first", first, (m, k)))
+            if not (k == 0 and ORDERS[m][0]):
+                steps.append((base + HOP, "second", second, (m, k)))
+            steps.append((base + 2 * HOP, "third", third, (m, k)))
+            end = max(end, base + 2 * HOP + CROSS, NORM_AT[-1] + 0.01 * (k + 1))
+            steps.append((end, "times", multiply, (m, k)))
+        steps.append((end + 0.001, "trade", exchange, (m,)))
+    for _, _, call, arguments in sorted(steps, key=lambda step: step[0]):
+        call(*arguments)
 
     query = queries[...].astype(jnp.float32)
     query = jnp.concatenate([query[:, g * head_size:(g + 1) * head_size] for g in range(heads)], axis=0)
@@ -271,6 +283,11 @@
         copy.wait_send()
 
 
+def hand_over(cache, read, cache_out, read_out):
+    cache_out[...] = cache[...]
+    read_out[...] = read[...]
+
+
 def copies(grid):
     depth, inner, groups, sections = grid
     pieces = depth * inner * groups
@@ -301,7 +318,7 @@
             pltpu.VMEM((rows, width), jnp.bfloat16),
             pltpu.VMEM((rows, width), jnp.bfloat16),
             pltpu.VMEM((2, width, columns), jnp.bfloat16),
-            pltpu.VMEM((rows, columns), jnp.float32),
+            pltpu.VMEM((2, rows, columns), jnp.float32),
             pltpu.VMEM((2, seats, sub // 2, 2 * head_size), jnp.bfloat16),
             pltpu.VMEM((2, seats, sub // 2, 2 * head_size), jnp.bfloat16),
             pltpu.VMEM((sections, heads, 2 * head_size), jnp.float32),
@@ -313,8 +330,13 @@
         compiler_params=pltpu.CompilerParams(
             collective_id=0, has_side_effects=True, vmem_limit_bytes=60 * 1024 * 1024
         ),
-    )(tokens.reshape(rows, width), ln_gain.reshape(1, width), w_key, w_value, queries, head_shift, key_shift)
-    return cache, read
+    )(tokens.reshape(rows, width), ln_gain, w_key, w_value, queries, head_shift, key_shift)
+    return pl.pallas_call(
+        hand_over,
+        out_shape=(jax.ShapeDtypeStruct(cache.shape, cache.dtype), jax.ShapeDtypeStruct(read.shape, read.dtype)),
+        in_specs=[vmem, vmem],
+        out_specs=(vmem, vmem),
+    )(cache, read)
 
 
 def solution(mesh):

time: 52.1 us -> 46.9 us (0.900)
  local copies, waits for them, and re-layouts: 4.43 us -> 0 us
  Pallas kernels: 46.7 us -> 45.9 us
    unnamed x2 -> x0, local copies, waits for them, and re-layouts: 3.12 us -> none
    pallas_call x1, Pallas kernels: 46.7 us -> 44 us  [local(): pl.pallas_call(functools.partial(body, grid, head_size), out_shape=(jax.S...]
    pallas_call x0 -> x1, Pallas kernels: none -> 1.87 us  [local(): pl.pallas_call(hand_over, out_shape=(jax.ShapeDtypeStruct(cache.shape, ca...]
    reshape x1 -> x0, local copies, waits for them, and re-layouts: 1.31 us -> none  [local(): ln_gain.reshape(1, width)]
where the time goes in v2:
time: 46.9 us; the launch traced here: 46.6 us
  Pallas kernels  45.9 us (98%)
  between operations  0.64 us (1%)
    pallas_call x1, Pallas kernels, local(): pl.pallas_call(functools.partial(body, grid, head_size), out_shape=(jax.S...  44 us
    pallas_call x1, Pallas kernels, local(): pl.pallas_call(hand_over, out_shape=(jax.ShapeDtypeStruct(cache.shape, ca...  1.87 us

profile of v2, /device:TPU:0, one launch (start us, length us, event | category | flops | bytes accessed | tf_op | source)
XLA Modules:
  0.0 46.6 jit_solution(15329165219051864417)
XLA Ops:
  0.6 44.0 %shard_map.86 = (bf16[1,2048,128]{2,1,0:T(8,128)(2,1)}, f32[1,512]{1,0:T(1,128)}) custom-call(bf16[512,4096]{1,0:T(8,128)(2,1)} %bitcast.1, bf16[4096]{0:T(1024)(128)(2,1)} %gain.1, bf16[512,256]{1,0:T(8,128)(2,1)} %w_key.1, bf16[512,256]{1,0:T(8,128)(2,1)} %w_value.1, bf16[1,512]{1,0:T(2,128)(2,1)} %queries.1, f32[4,8]{1,0:T(4,128)} %head_shift.1, ...), custom_call_target="tpu_custom_call" | custom-call | tf_op jit(solution)/shard_map/pallas_call | solution.py:309
  44.7 1.9 %shard_map.87 = (bf16[1,2048,128]{2,1,0:T(8,128)(2,1)}, f32[1,512]{1,0:T(1,128)}) custom-call(bf16[1,2048,128]{2,1,0:T(8,128)(2,1)} %get-tuple-element.4.cache, f32[1,512]{1,0:T(1,128)} %get-tuple-element.5.read), custom_call_target="tpu_custom_call" | custom-call | tf_op jit(solution)/shard_map/pallas_call | solution.py:334
